TPU v7x, 32 devices: a whole 2x2x4 slice. The times are simulated.
32 devices in a mesh: ep: 4 (over y, x), tp: 8 (over z, core).
Axes of the slice: x: 2, y: 2, z: 4, core: 2. Of those that a mesh axis runs over, the one named last changes fastest.
Arguments:
- queries: bfloat16 [2048, 16, 128], P('ep', 'tp'), may hold values from -300 to 300
- keys: bfloat16 [2048, 16, 128], P('ep', 'tp'), may hold values from -4 to 4
- values: bfloat16 [2048, 16, 128], P('ep', 'tp'), may hold values from -6 to 6
- mix_weight: float32 [16], P('tp'), may hold values from 0.3 to 0.8
- sub_gain: float32 [128], replicated, may hold values from 0.1 to 1.9
- tokens: bfloat16 [1024, 2048], P('ep', 'tp'), may hold values from -6 to 6
- routes: int32 [1024, 2], P('ep'), may hold values from 0 to 7, all different within a row; in each aligned block of 256 rows (0 to 255, 256 to 511, ...) at most 96 rows name the same one
- route_weights: float32 [1024, 2], P('ep'), may hold values from 0.1 to 1
- expert_gain: float32 [2048], replicated, may hold values from 0.1 to 1.9
- gate_weight: bfloat16 [8, 2048, 4096], P('ep', None, 'tp'), may hold values from -0.375 to 0.375
- up_weight: bfloat16 [8, 2048, 4096], P('ep', None, 'tp'), may hold values from -0.375 to 0.375
- down_weight: bfloat16 [8, 4096, 2048], P('ep', 'tp'), may hold values from -0.09375 to 0.09375
Outputs:
- attn_out: bfloat16 [2048, 16, 128], P('ep', 'tp')
- moe_out: bfloat16 [1024, 2048], P('ep', 'tp')
Inputs may be any that keep to these rules, and one draw needn't show every extreme that they name: `routes`: in each aligned block of 256 rows no expert is named by more than 96 rows, and in every draw some expert is named by exactly 96 rows of some block.
All inputs are finite; a program needn't handle non-finite values.
Results may differ from a plain program's by a relative error of at most 0.018.
Values may be sent and summed in bfloat16 or wider, within the bound.
A program may use at most 128 MiB of HBM per device.

v0:
```python
import functools

import jax
import jax.numpy as jnp
from jax import lax
from jax.experimental import pallas as pl
from jax.experimental.pallas import tpu as pltpu
from jax.sharding import PartitionSpec as P

NEG_FILL = -1e30
SUB_EPS = 1e-05
NORM_EPS = 1e-06
CLAMP_LIMIT = 7.0
GLU_ALPHA = 1.702
OUT_SCALE = 0.8
CORES = 2
F32 = jnp.float32
BF16 = jnp.bfloat16
MESH = pl.DeviceIdType.MESH


def dot(a, b):
    return jnp.dot(a, b, preferred_element_type=F32)


def dot_t(a, b):
    return lax.dot_general(a, b, (((1,), (1,)), ((), ())), preferred_element_type=F32)


def loop(lower, upper, body):
    def step(index, carry):
        body(index)
        return carry

    lax.fori_loop(lower, upper, step, 0)


def layer_kernel(
    n_ep, n_tp, cap, heads, rank_pad,
    tok, routes_t, route_w_t, gain, gate_hbm, up_hbm, down_hbm, q_in, k_in, v_in, mix, sub_gain,
    attn_out, moe_out,
    gate, up, down, held, outgoing, arrived, normed, squares, gate_sum, up_sum, hidden, part, pair,
    up_stage, up_got, dn_stage, dn_got, total, final, back, q, kv, kv_all,
    top, norm_sum, weighted,
    w_sem, ag_s, ag_r, dp_s, dp_r, fw_s, fw_r, kv_s, kv_r, pr_s, pr_r,
    up_s, up_r, dn_s, dn_r, rt_s, rt_r,
):
    e, t = lax.axis_index("ep"), lax.axis_index("tp")
    nz = n_tp // CORES
    z, c = t // CORES, t % CORES
    partner = t + 1 - 2 * c
    rows, shard = tok.shape
    local = gate_hbm.shape[0]
    experts = n_ep * local
    pad = rank_pad
    slots = experts * pad
    block = local * pad
    has_up, has_dn = z < nz - 1, z > 0

    weights = [
        pltpu.make_async_copy(source, target, w_sem.at[i])
        for i, (source, target) in enumerate(((gate_hbm, gate), (up_hbm, up), (down_hbm, down)))
    ]
    for copy in weights:
        copy.start()

    barrier = pltpu.get_barrier_semaphore()
    pl.semaphore_signal(barrier, inc=1, device_id=(e, partner), device_id_type=MESH)

    @pl.when(has_up)
    def _():
        pl.semaphore_signal(barrier, inc=1, device_id=(e, t + CORES), device_id_type=MESH)

    @pl.when(has_dn)
    def _():
        pl.semaphore_signal(barrier, inc=1, device_id=(e, t - CORES), device_id_type=MESH)

    loop(1, n_ep, lambda d: pl.semaphore_signal(
        barrier, inc=1, device_id=((e + d) % n_ep, t), device_id_type=MESH))
    pl.semaphore_wait(barrier, n_ep + has_up.astype(jnp.int32) + has_dn.astype(jnp.int32))

    def send(source, target, s_sem, r_sem, device):
        return pltpu.make_async_remote_copy(
            src_ref=source, dst_ref=target, send_sem=s_sem, recv_sem=r_sem,
            device_id=device, device_id_type=MESH)

    def shard_copy(way, r, origin):
        source = tok if r == 0 else held.at[origin]
        target = t + CORES if way == 0 else t - CORES
        return send(source, held.at[origin], ag_s.at[way, r], ag_r.at[way, r], (e, target))

    def shard_sends(r):
        @pl.when(has_up & (z - r >= 0))
        def _():
            shard_copy(0, r, z - r).start()

        @pl.when(has_dn & (z + r < nz))
        def _():
            shard_copy(1, r, z + r).start()

    def shard_send_waits(r):
        @pl.when(has_up & (z - r >= 0))
        def _():
            shard_copy(0, r, z - r).wait_send()

        @pl.when(has_dn & (z + r < nz))
        def _():
            shard_copy(1, r, z + r).wait_send()

    shard_sends(0)

    row_i = lax.broadcasted_iota(jnp.int32, (rows, rows), 0)
    col_i = lax.broadcasted_iota(jnp.int32, (rows, rows), 1)
    picks = routes_t.shape[0]
    exp_row = lax.broadcasted_iota(jnp.int32, (experts, rows), 0)
    hot_t = [(routes_t[p:p + 1, :] == exp_row).astype(F32) for p in range(picks)]
    before_t = dot(sum(hot_t).astype(BF16), (row_i < col_i).astype(F32).astype(BF16))
    slot_row = [
        jnp.sum(h * (before_t + (exp_row * pad).astype(F32)), axis=0, keepdims=True)
        for h in hot_t
    ]
    slot_i = lax.broadcasted_iota(jnp.int32, (slots, rows), 0).astype(F32)

    def as_column(line):
        return jnp.transpose(jnp.broadcast_to(line, (128, rows)))[:, :1]

    choose = sum((slot_i == s).astype(F32) for s in slot_row).astype(BF16)

    def piece(k, d):
        source = outgoing.at[k, (e + d) % n_ep]
        return send(source, arrived.at[CORES * k + c, e], dp_s.at[k, d - 1], dp_r.at[k, d - 1],
                    ((e + d) % n_ep, t))

    def incoming(k, d):
        origin = (e + n_ep - d) % n_ep
        return send(outgoing.at[k, origin], arrived.at[CORES * k + c, origin],
                    dp_s.at[k, d - 1], dp_r.at[k, d - 1], (origin, t))

    def forward(k, d):
        origin = (e + n_ep - d) % n_ep
        place = arrived.at[CORES * k + c, origin]
        return send(place, place, fw_s.at[k, d], fw_r.at[k, d], (e, partner))

    def forwarded(k, d):
        origin = (e + n_ep - d) % n_ep
        place = arrived.at[CORES * k + 1 - c, origin]
        return send(place, place, fw_s.at[k, d], fw_r.at[k, d], (e, partner))

    def dispatch(k, source):
        made = dot(choose, source).astype(BF16).reshape(n_ep, block, shard)
        outgoing[k] = made
        arrived[CORES * k + c, e] = outgoing[k, e]
        loop(1, n_ep, lambda d: piece(k, d).start())
        forward(k, 0).start()

    dispatch(z, tok[...])
    for r in range(nz - 1):
        got_up = has_dn & (z - 1 - r >= 0)
        got_dn = has_up & (z + 1 + r < nz)

        @pl.when(got_up)
        def _():
            shard_copy(0, r, z - 1 - r).wait_recv()

        @pl.when(got_dn)
        def _():
            shard_copy(1, r, z + 1 + r).wait_recv()

        if r < nz - 2:
            shard_sends(r + 1)

        @pl.when(got_up)
        def _():
            dispatch(z - 1 - r, held[z - 1 - r])

        @pl.when(got_dn)
        def _():
            dispatch(z + 1 + r, held[z + 1 + r])

    items = q.shape[1]
    pick_i = lax.broadcasted_iota(jnp.int32, (items, items * heads), 0)
    from_i = lax.broadcasted_iota(jnp.int32, (items, items * heads), 1)
    for h in range(heads):
        take = (from_i == pick_i * heads + h).astype(F32).astype(BF16)
        q[h] = dot(take, q_in[...]).astype(BF16)
        kv[0, h] = dot(take, k_in[...]).astype(BF16)
        kv[1, h] = dot(take, v_in[...]).astype(BF16)

    def kv_copy(d):
        return send(kv, kv_all.at[e], kv_s.at[d - 1], kv_r.at[d - 1], ((e + d) % n_ep, t))

    def kv_got(d):
        origin = (e + n_ep - d) % n_ep
        return send(kv, kv_all.at[origin], kv_s.at[d - 1], kv_r.at[d - 1], (origin, t))

    loop(1, n_ep - e, lambda d: kv_copy(d).start())

    length, width = q.shape[1:]
    lane = lax.broadcasted_iota(jnp.int32, (length, width), 1)
    scale = (width // 2) ** -0.5

    def attend(keys_values, diagonal):
        for h in range(heads):
            key, value = keys_values[0, h], keys_values[1, h]
            scaled_q = q[h].astype(F32) * scale
            for m in range(2):
                n = 2 * h + m
                mine = (lane < width // 2) if m == 0 else (lane >= width // 2)
                query = jnp.where(mine, scaled_q, 0.0).astype(BF16)
                scores = dot_t(query, key)
                if diagonal:
                    q_pos = lax.broadcasted_iota(jnp.int32, scores.shape, 0)
                    k_pos = lax.broadcasted_iota(jnp.int32, scores.shape, 1)
                    scores = jnp.where(k_pos <= q_pos, scores, NEG_FILL)
                high = jnp.max(scores, axis=1, keepdims=True)
                if not diagonal:
                    old = top[n]
                    high = jnp.maximum(high, old)
                    shrink = jnp.exp(old - high)
                w = jnp.exp(scores - high)
                s = jnp.sum(w, axis=1, keepdims=True)
                v = dot(w.astype(BF16), value)
                top[n] = high
                norm_sum[n] = s if diagonal else norm_sum[n] * shrink + s
                weighted[n] = v if diagonal else weighted[n] * shrink + v

    def attend_far(lower, upper):
        def body(d):
            kv_got(d).wait_recv()
            attend(kv_all.at[(e + n_ep - d) % n_ep], False)

        loop(lower, jnp.minimum(upper, e + 1), body)

    attend(kv, True)

    def pass_on(k):
        def body(d):
            incoming(k, d).wait_recv()
            forward(k, d).start()

        loop(1, n_ep, body)

    for copy in weights:
        copy.wait()
    gate_sum[...] = jnp.zeros_like(gate_sum)
    up_sum[...] = jnp.zeros_like(up_sum)
    squares[...] = jnp.zeros_like(squares)
    width_total = gain.shape[2] * n_tp
    deep = CORES * shard

    def absorb(k):
        loop(0, n_ep, lambda d: forwarded(k, d).wait_recv())

        def prepare(source):
            place = pl.ds(pl.multiple_of(source * pad, pad), pad)
            for x in range(local):
                for half in range(CORES):
                    floats = arrived[CORES * k + half, source, x * pad:(x + 1) * pad, :].astype(F32)
                    squares[x, place, :] += floats * floats
                    normed[x, place, half * shard:(half + 1) * shard] = (
                        floats * gain[CORES * k + half]).astype(BF16)

        loop(0, n_ep, prepare)
        depth = pl.ds(pl.multiple_of(k * deep, deep), deep)
        for x in range(local):
            gate_sum[x] += dot(normed[x], gate[x, depth, :])
            up_sum[x] += dot(normed[x], up[x, depth, :])

    def visit(i, action):
        k = z - (i + 1) // 2 * (i % 2) + i // 2 * (1 - i % 2)

        @pl.when((k >= 0) & (k < nz))
        def _():
            action(k)

    def arrival(i):
        @pl.when(i < 2 * nz - 1)
        def _():
            visit(i, pass_on)

        @pl.when(i >= 2)
        def _():
            visit(i - 2, absorb)

    loop(0, 2 * nz + 1, arrival)

    count = n_ep * pad
    for x in range(local):
        mean = jnp.sum(squares[x], axis=1, keepdims=True) / width_total
        factor = lax.rsqrt(mean + NORM_EPS)
        gate_pre = jnp.minimum(gate_sum[x] * factor, CLAMP_LIMIT)
        up_pre = jnp.clip(up_sum[x] * factor, -CLAMP_LIMIT, CLAMP_LIMIT)
        hidden[...] = ((up_pre + 1.0) * gate_pre * jax.nn.sigmoid(GLU_ALPHA * gate_pre)).astype(BF16)
        for k in range(n_tp):
            product = dot(hidden[...], down[x, :, k * shard:(k + 1) * shard])
            part[k % CORES, x, k // CORES] = product.astype(BF16)
        send(part.at[1 - c, x], pair.at[x], pr_s.at[x], pr_r.at[x], (e, partner)).start()

    def own(d, x):
        return part[c, x, d].astype(F32) + pair[x, d].astype(F32)

    def sum_copy(way, r, x):
        if way == 0:
            return send(up_stage.at[r, x], up_got.at[r, x], up_s.at[r, x], up_r.at[r, x],
                        (e, t + CORES))
        return send(dn_stage.at[r, x], dn_got.at[r, x], dn_s.at[r, x], dn_r.at[r, x],
                    (e, t - CORES))

    for r in range(nz - 1):
        for x in range(local):
            if r == 0:
                send(part.at[1 - c, x], pair.at[x], pr_s.at[x], pr_r.at[x], (e, partner)).wait_recv()
            for way in range(2):
                place = z if way == 0 else nz - 1 - z
                goal = nz - 1 - r + z if way == 0 else r - (nz - 1) + z
                stage, got = (up_stage, up_got) if way == 0 else (dn_stage, dn_got)

                @pl.when((place == 0) & (nz > 1))
                def _():
                    stage[r, x] = own(goal, x).astype(BF16)
                    sum_copy(way, r, x).start()

                if r > 0:
                    @pl.when((place > 0) & (place <= r))
                    def _():
                        sum_copy(way, r - 1, x).wait_recv()
                        stage[r, x] = (own(goal, x) + got[r - 1, x].astype(F32)).astype(BF16)
                        sum_copy(way, r, x).start()

        if r > 0:
            attend_far(1 + (n_ep - 1) * (r - 1) // (nz - 1), 1 + (n_ep - 1) * r // (nz - 1))

    last = nz - 2
    for x in range(local):
        total[...] = own(z, x)

        @pl.when(has_dn)
        def _():
            sum_copy(0, last, x).wait_recv()
            total[...] += up_got[last, x].astype(F32)

        @pl.when(has_up)
        def _():
            sum_copy(1, last, x).wait_recv()
            total[...] += dn_got[last, x].astype(F32)

        for source in range(n_ep):
            final[source, x * pad:(x + 1) * pad, :] = (
                total[source * pad:(source + 1) * pad, :].astype(BF16))

    def give(d):
        return send(final.at[(e + d) % n_ep], back.at[e], rt_s.at[d - 1], rt_r.at[d - 1],
                    ((e + d) % n_ep, t))

    def given(d):
        origin = (e + n_ep - d) % n_ep
        return send(final.at[origin], back.at[origin], rt_s.at[d - 1], rt_r.at[d - 1], (origin, t))

    loop(1, n_ep, lambda d: give(d).start())
    back[e] = final[e]

    attend_far(1 + (n_ep - 1) * (nz - 2) // (nz - 1), n_ep)
    for h in range(heads):
        first = weighted[2 * h] / norm_sum[2 * h]
        second = weighted[2 * h + 1] / norm_sum[2 * h + 1]
        blend = first - mix[h] * second
        mean = jnp.mean(blend * blend, axis=1, keepdims=True)
        scaled = (blend * lax.rsqrt(mean + SUB_EPS) * sub_gain[...] * OUT_SCALE).astype(BF16)
        put_i = lax.broadcasted_iota(jnp.int32, (items * heads, items), 0)
        of_i = lax.broadcasted_iota(jnp.int32, (items * heads, items), 1)
        placed = dot((put_i == of_i * heads + h).astype(F32).astype(BF16), scaled)
        woven = placed if h == 0 else woven + placed
    attn_out[...] = woven.astype(BF16)

    lane_slot = lax.broadcasted_iota(jnp.int32, (rows, slots), 1).astype(F32)
    loop(1, n_ep, lambda d: given(d).wait_recv())
    results = back[...].reshape(slots, shard)
    mixed = jnp.zeros((rows, shard), F32)
    for p in range(picks):
        selected = dot((lane_slot == as_column(slot_row[p])).astype(F32).astype(BF16), results)
        mixed = mixed + selected * as_column(route_w_t[p:p + 1, :])
    moe_out[...] = mixed.astype(BF16)

    for r in range(nz - 1):
        shard_send_waits(r)
    loop(0, nz, lambda k: loop(1, n_ep, lambda d: piece(k, d).wait_send()))
    loop(0, nz, lambda k: loop(0, n_ep, lambda d: forward(k, d).wait_send()))
    loop(1, n_ep - e, lambda d: kv_copy(d).wait_send())
    loop(1, n_ep, lambda d: give(d).wait_send())
    for x in range(local):
        send(part.at[1 - c, x], pair.at[x], pr_s.at[x], pr_r.at[x], (e, partner)).wait_send()
        for r in range(nz - 1):
            for way in range(2):
                place = z if way == 0 else nz - 1 - z

                @pl.when(place <= r)
                def _():
                    sum_copy(way, r, x).wait_send()


def make_shards(n_ep, n_tp):
    def shards(
        queries, keys, values, mix_weight, sub_gain, tokens, routes, route_weights,
        expert_gain, gate_weight, up_weight, down_weight,
    ):
        rows, shard = tokens.shape
        picks = routes.shape[1]
        local, depth, units = gate_weight.shape
        cap = 3 * rows * picks // (2 * n_ep * local)
        pad = -(-cap // 16) * 16
        length, heads, width = queries.shape
        value_width = values.shape[2]
        nz = n_tp // CORES
        block = local * pad
        count = n_ep * pad
        vmem = pl.BlockSpec(memory_space=pltpu.VMEM)
        smem = pl.BlockSpec(memory_space=pltpu.SMEM)
        hbm = pl.BlockSpec(memory_space=pl.ANY)
        dma = pltpu.SemaphoreType.DMA
        peers = n_ep - 1
        attn, moe = pl.pallas_call(
            functools.partial(layer_kernel, n_ep, n_tp, cap, heads, pad),
            out_shape=(
                jax.ShapeDtypeStruct((length * heads, value_width), BF16),
                jax.ShapeDtypeStruct((rows, shard), BF16),
            ),
            in_specs=[vmem] * 4 + [hbm] * 3 + [vmem, vmem, vmem, smem, vmem],
            out_specs=(vmem, vmem),
            scratch_shapes=[
                pltpu.VMEM(gate_weight.shape, BF16),
                pltpu.VMEM(up_weight.shape, BF16),
                pltpu.VMEM(down_weight.shape, BF16),
                pltpu.VMEM((nz, rows, shard), BF16),
                pltpu.VMEM((nz, n_ep, block, shard), BF16),
                pltpu.VMEM((n_tp, n_ep, block, shard), BF16),
                pltpu.VMEM((local, count, CORES * shard), BF16),
                pltpu.VMEM((local, count, shard), F32),
                pltpu.VMEM((local, count, units), F32),
                pltpu.VMEM((local, count, units), F32),
                pltpu.VMEM((count, units), BF16),
                pltpu.VMEM((CORES, local, nz, count, shard), BF16),
                pltpu.VMEM((local, nz, count, shard), BF16),
            ]
            + [pltpu.VMEM((nz - 1, local, count, shard), BF16)] * 4
            + [
                pltpu.VMEM((count, shard), F32),
                pltpu.VMEM((n_ep, block, shard), BF16),
                pltpu.VMEM((n_ep, block, shard), BF16),
                pltpu.VMEM((heads, length, width), BF16),
                pltpu.VMEM((2, heads, length, width), BF16),
                pltpu.VMEM((n_ep, 2, heads, length, width), BF16),
                pltpu.VMEM((2 * heads, length, 1), F32),
                pltpu.VMEM((2 * heads, length, 1), F32),
                pltpu.VMEM((2 * heads, length, value_width), F32),
                dma((3,)),
                dma((2, nz - 1)), dma((2, nz - 1)),
                dma((nz, peers)), dma((nz, peers)),
                dma((nz, n_ep)), dma((nz, n_ep)),
                dma((peers,)), dma((peers,)),
                dma((local,)), dma((local,)),
                dma((nz - 1, local)), dma((nz - 1, local)),
                dma((nz - 1, local)), dma((nz - 1, local)),
                dma((peers,)), dma((peers,)),
            ],
            compiler_params=pltpu.CompilerParams(
                collective_id=0, has_side_effects=True, vmem_limit_bytes=60 * 2**20),
            name="layer",
        )(
            tokens, jnp.transpose(routes), jnp.transpose(route_weights),
            expert_gain.reshape(n_tp, 1, shard), gate_weight, up_weight, down_weight,
            queries.reshape(length * heads, width), keys.reshape(length * heads, width),
            values.reshape(length * heads, value_width), mix_weight, sub_gain[None, :],
        )
        return attn.reshape(length, heads, value_width), moe

    return shards


def solution(mesh):
    return jax.shard_map(
        make_shards(mesh.shape["ep"], mesh.shape["tp"]),
        mesh=mesh,
        in_specs=(
            P("ep", "tp", None),
            P("ep", "tp", None),
            P("ep", "tp", None),
            P("tp"),
            P(),
            P("ep", "tp"),
            P("ep", None),
            P("ep", None),
            P(),
            P("ep", None, "tp"),
            P("ep", None, "tp"),
            P("ep", "tp", None),
        ),
        out_specs=(P("ep", "tp", None), P("ep", "tp")),
        check_vma=False,
    )
```

profile of v0, /device:TPU:18, one launch (start us, length us, event | category | flops | bytes accessed | tf_op | source)
XLA Modules:
  0.0 80.5 jit_solution(809462410916217389)
XLA Ops:
  0.6 76.5 %layer.1 = (bf16[1024,128]{1,0:T(8,128)(2,1)}, bf16[256,256]{1,0:T(8,128)(2,1)}) custom-call(bf16[256,256]{1,0:T(8,128)(2,1)} %tok.1, s32[2,256]{1,0:T(2,128)} %bitcast.13, f32[2,256]{1,0:T(2,128)} %bitcast.14, f32[8,1,256]{2,1,0:T(1,128)} %bitcast.12, bf16[2,2048,512]{2,1,0:T(8,128)(2,1)} %gate_hbm.1, bf16[2,2048,512]{2,1,0:T(8,128)(2,1)} %up_hbm.1, ...), custom_call_target="tpu_custom_call" | custom-call | tf_op jit(solution)/shard_map/layer/pallas_call | solution.py:421
  77.1 1.8 %copy.16 = bf16[512,2,128]{2,1,0:T(2,128)(2,1)} copy(bf16[512,2,128]{2,1,0:T(2,128)(2,1)} %bitcast.11) | data formatting | bytes 524288
  79.0 1.6 %copy.17 = bf16[256,256]{1,0:T(8,128)(2,1)} copy(bf16[256,256]{1,0:T(8,128)(2,1)} %get-tuple-element.9) | data formatting | bytes 262144
where the time goes:
time: 80.7 us; the launch traced here: 80.5 us
  Pallas kernels  76.5 us (95%)
  local copies, waits for them, and re-layouts  3.4 us (4%)
    pallas_call x1, Pallas kernels, shards(): pl.pallas_call(functools.partial(layer_kernel, n_ep, n_tp, cap, heads, pa...  76.5 us
    unnamed x2, local copies, waits for them, and re-layouts  3.4 us

commit v1 on v0

v1 whole, which is shorter than its diff:
```python
import functools

import jax
import jax.numpy as jnp
from jax import lax
from jax.experimental import pallas as pl
from jax.experimental.pallas import tpu as pltpu
from jax.sharding import PartitionSpec as P

NEG_FILL = -1e30
SUB_EPS = 1e-05
NORM_EPS = 1e-06
CLAMP_LIMIT = 7.0
GLU_ALPHA = 1.702
OUT_SCALE = 0.8
CORES = 2
F32 = jnp.float32
BF16 = jnp.bfloat16
MESH = pl.DeviceIdType.MESH


def dot(a, b):
    return jnp.dot(a, b, preferred_element_type=F32)


def dot_t(a, b):
    return lax.dot_general(a, b, (((1,), (1,)), ((), ())), preferred_element_type=F32)


def loop(lower, upper, body):
    def step(index, carry):
        body(index)
        return carry

    lax.fori_loop(lower, upper, step, 0)


def layer_kernel(
    n_ep, n_tp, cap, heads, rank_pad,
    tok_hbm, routes_hbm, route_w_hbm, gain_hbm, gate_hbm, up_hbm, down_hbm,
    q_hbm, k_hbm, v_hbm, sub_gain_hbm, mix,
    attn_out, moe_out,
    tok, routes_t, route_w_t, gain, q_in, k_in, v_in, sub_gain,
    gate, up, down, held, outgoing, arrived, normed, squares, gate_sum, up_sum, hidden, part, pair,
    fin, ex, slot_got, tok_stage, tok_got, held_sum, final, back, pick, pick_w, q, kv, kv_all,
    top, norm_sum, weighted,
    in_sem, w_sem, ag_s, ag_r, dp_s, dp_r, fw_s, fw_r, kv_s, kv_r, kh_s, kh_r, pr_s, pr_r,
    ex_s, ex_r, sl_s, sl_r, tk_s, tk_r, rt_s, rt_r,
):
    e, t = lax.axis_index("ep"), lax.axis_index("tp")
    nz = n_tp // CORES
    z, c = t // CORES, t % CORES
    partner = t + 1 - 2 * c
    rows, shard = tok.shape
    local = gate_hbm.shape[0]
    experts = n_ep * local
    pad = rank_pad
    slots = experts * pad
    block = local * pad
    has_up, has_dn = z < nz - 1, z > 0

    loads = [
        pltpu.make_async_copy(source, target, in_sem.at[i])
        for i, (source, target) in enumerate((
            (tok_hbm, tok), (routes_hbm, routes_t), (route_w_hbm, route_w_t), (gain_hbm, gain),
            (q_hbm, q_in), (k_hbm, k_in), (v_hbm, v_in), (sub_gain_hbm, sub_gain)))
    ]
    for copy in loads:
        copy.start()
    weights = [
        pltpu.make_async_copy(source, target, w_sem.at[i])
        for i, (source, target) in enumerate(((gate_hbm, gate), (up_hbm, up), (down_hbm, down)))
    ]
    for copy in weights:
        copy.start()

    barrier = pltpu.get_barrier_semaphore()
    pl.semaphore_signal(barrier, inc=1, device_id=(e, partner), device_id_type=MESH)

    @pl.when(has_up)
    def _():
        pl.semaphore_signal(barrier, inc=1, device_id=(e, t + CORES), device_id_type=MESH)

    @pl.when(has_dn)
    def _():
        pl.semaphore_signal(barrier, inc=1, device_id=(e, t - CORES), device_id_type=MESH)

    loop(1, n_ep, lambda d: pl.semaphore_signal(
        barrier, inc=1, device_id=((e + d) % n_ep, t), device_id_type=MESH))
    for copy in loads[:2]:
        copy.wait()
    with jax.named_scope("barrier"):
        pl.semaphore_wait(barrier, n_ep + has_up.astype(jnp.int32) + has_dn.astype(jnp.int32))

    def send(source, target, s_sem, r_sem, device):
        return pltpu.make_async_remote_copy(
            src_ref=source, dst_ref=target, send_sem=s_sem, recv_sem=r_sem,
            device_id=device, device_id_type=MESH)

    def shard_copy(way, r, origin):
        source = tok if r == 0 else held.at[origin]
        target = t + CORES if way == 0 else t - CORES
        return send(source, held.at[origin], ag_s.at[way, r], ag_r.at[way, r], (e, target))

    def shard_sends(r):
        @pl.when(has_up & (z - r >= 0))
        def _():
            shard_copy(0, r, z - r).start()

        @pl.when(has_dn & (z + r < nz))
        def _():
            shard_copy(1, r, z + r).start()

    def shard_send_waits(r):
        @pl.when(has_up & (z - r >= 0))
        def _():
            shard_copy(0, r, z - r).wait_send()

        @pl.when(has_dn & (z + r < nz))
        def _():
            shard_copy(1, r, z + r).wait_send()

    shard_sends(0)

    row_i = lax.broadcasted_iota(jnp.int32, (rows, rows), 0)
    col_i = lax.broadcasted_iota(jnp.int32, (rows, rows), 1)
    picks = routes_t.shape[0]
    exp_row = lax.broadcasted_iota(jnp.int32, (experts, rows), 0)
    hot_t = [(routes_t[p:p + 1, :] == exp_row).astype(F32) for p in range(picks)]
    before_t = dot(sum(hot_t).astype(BF16), (row_i < col_i).astype(F32).astype(BF16))
    slot_row = [
        jnp.sum(h * (before_t + (exp_row * pad).astype(F32)), axis=0, keepdims=True)
        for h in hot_t
    ]
    slot_i = lax.broadcasted_iota(jnp.int32, (slots, rows), 0).astype(F32)

    def as_column(line):
        return jnp.transpose(jnp.broadcast_to(line, (128, rows)))[:, :1]

    choose = sum((slot_i == s).astype(F32) for s in slot_row).astype(BF16)

    def piece(k, d):
        source = outgoing.at[k, (e + d) % n_ep]
        return send(source, arrived.at[CORES * k + c, e], dp_s.at[k, d - 1], dp_r.at[k, d - 1],
                    ((e + d) % n_ep, t))

    def incoming(k, d):
        origin = (e + n_ep - d) % n_ep
        return send(outgoing.at[k, origin], arrived.at[CORES * k + c, origin],
                    dp_s.at[k, d - 1], dp_r.at[k, d - 1], (origin, t))

    def forward(k, d):
        origin = (e + n_ep - d) % n_ep
        place = arrived.at[CORES * k + c, origin]
        return send(place, place, fw_s.at[k, d], fw_r.at[k, d], (e, partner))

    def forwarded(k, d):
        origin = (e + n_ep - d) % n_ep
        place = arrived.at[CORES * k + 1 - c, origin]
        return send(place, place, fw_s.at[k, d], fw_r.at[k, d], (e, partner))

    def dispatch(k, source):
        made = dot(choose, source).astype(BF16).reshape(n_ep, block, shard)
        outgoing[k] = made
        arrived[CORES * k + c, e] = outgoing[k, e]
        loop(1, n_ep, lambda d: piece(k, d).start())
        forward(k, 0).start()

    items = q.shape[1]

    def unpack():
        for copy in loads[2:]:
            copy.wait()
        pick_i = lax.broadcasted_iota(jnp.int32, (items, items * heads), 0)
        from_i = lax.broadcasted_iota(jnp.int32, (items, items * heads), 1)
        for h in range(heads):
            take = (from_i == pick_i * heads + h).astype(F32).astype(BF16)
            q[h] = dot(take, q_in[...]).astype(BF16)
            kv[0, h] = dot(take, k_in[...]).astype(BF16)
            kv[1, h] = dot(take, v_in[...]).astype(BF16)

    def pick_tables():
        lane_slot = lax.broadcasted_iota(jnp.int32, (rows, slots), 1).astype(F32)
        for p in range(picks):
            pick[p] = (lane_slot == as_column(slot_row[p])).astype(F32).astype(BF16)
            pick_w[p] = jnp.transpose(jnp.broadcast_to(route_w_t[p:p + 1, :], (128, rows)))

    length, width = q.shape[1:]
    lane = lax.broadcasted_iota(jnp.int32, (length, width), 1)
    scale = (width // 2) ** -0.5

    def attend(keys_values, diagonal):
        for h in range(heads):
            key, value = keys_values[0, h], keys_values[1, h]
            scaled_q = q[h].astype(F32) * scale
            for m in range(2):
                n = 2 * h + m
                mine = (lane < width // 2) if m == 0 else (lane >= width // 2)
                query = jnp.where(mine, scaled_q, 0.0).astype(BF16)
                scores = dot_t(query, key)
                if diagonal:
                    q_pos = lax.broadcasted_iota(jnp.int32, scores.shape, 0)
                    k_pos = lax.broadcasted_iota(jnp.int32, scores.shape, 1)
                    scores = jnp.where(k_pos <= q_pos, scores, NEG_FILL)
                high = jnp.max(scores, axis=1, keepdims=True)
                if not diagonal:
                    old = top[n]
                    high = jnp.maximum(high, old)
                    shrink = jnp.exp(old - high)
                w = jnp.exp(scores - high)
                s = jnp.sum(w, axis=1, keepdims=True)
                v = dot(w.astype(BF16), value)
                top[n] = high
                norm_sum[n] = s if diagonal else norm_sum[n] * shrink + s
                weighted[n] = v if diagonal else weighted[n] * shrink + v

    relay = n_ep == 4

    def kv_copy(d):
        return send(kv, kv_all.at[e], kv_s.at[d - 1], kv_r.at[e], ((e + d) % n_ep, t))

    def kv_got(origin):
        return send(kv, kv_all.at[origin], kv_s.at[0], kv_r.at[origin], (origin, t))

    def kv_direct(d, action):
        if relay and d == 1:
            @pl.when(e % 2 == 0)
            def _():
                action(kv_copy(d))
        elif relay and d == 2:
            @pl.when(e < 2)
            def _():
                action(kv_copy(d))
        elif not relay:
            @pl.when(e + d < n_ep)
            def _():
                action(kv_copy(d))

    def kv_half(origin, half, device):
        place = kv_all.at[origin, half]
        return send(place, place, kh_s.at[origin, half], kh_r.at[origin, half], (device, t))

    def kv_cross(action):
        if relay:
            @pl.when(e == 1)
            def _():
                action(send(kv.at[0], kv_all.at[1, 0], kh_s.at[1, 0], kh_r.at[1, 0], (2, t)))

    def kv_pass(origin, action):
        if relay:
            for half in range(2):
                @pl.when((e == half + 1) & (origin == 0))
                def _():
                    action(kv_half(0, half, 3))

            @pl.when((e == 3) & (origin == 1))
            def _():
                action(kv_half(1, 1, 2))

    def far_origin(j):
        if relay:
            return jnp.where(e == 3, (j + 1) % 3, j)
        return e - 1 - j

    def attend_far(lower, upper):
        def body(j):
            origin = far_origin(j)
            if relay:
                halves = ((e == 3) & (origin == 0)) | ((e == 2) & (origin == 1))

                @pl.when(halves)
                def _():
                    for half in range(2):
                        kv_half(origin, half, 3).wait_recv()

                @pl.when(jnp.logical_not(halves))
                def _():
                    kv_got(origin).wait_recv()
            else:
                kv_got(origin).wait_recv()
            kv_pass(origin, lambda copy: copy.start())
            attend(kv_all.at[origin], False)

        loop(lower, jnp.minimum(upper, e), body)

    with jax.named_scope("dispatch_own"):
        dispatch(z, tok[...])
    with jax.named_scope("unpack"):
        unpack()
    for r in range(nz - 1):
        got_up = has_dn & (z - 1 - r >= 0)
        got_dn = has_up & (z + 1 + r < nz)

        with jax.named_scope("shard_wait"):
            @pl.when(got_up)
            def _():
                shard_copy(0, r, z - 1 - r).wait_recv()

            @pl.when(got_dn)
            def _():
                shard_copy(1, r, z + 1 + r).wait_recv()

            if r < nz - 2:
                shard_sends(r + 1)

        with jax.named_scope("dispatch"):
            @pl.when(got_up)
            def _():
                dispatch(z - 1 - r, held[z - 1 - r])

            @pl.when(got_dn)
            def _():
                dispatch(z + 1 + r, held[z + 1 + r])

        if r == 0:
            with jax.named_scope("diag"):
                attend(kv, True)
    for d in range(1, n_ep):
        kv_direct(d, lambda copy: copy.start())
    kv_cross(lambda copy: copy.start())

    def pass_on(k):
        def body(d):
            incoming(k, d).wait_recv()
            forward(k, d).start()

        loop(1, n_ep, body)

    for copy in weights:
        copy.wait()
    gate_sum[...] = jnp.zeros_like(gate_sum)
    up_sum[...] = jnp.zeros_like(up_sum)
    squares[...] = jnp.zeros_like(squares)
    width_total = gain.shape[2] * n_tp
    deep = CORES * shard

    def absorb(k):
        loop(0, n_ep, lambda d: forwarded(k, d).wait_recv())

        def prepare(source):
            place = pl.ds(pl.multiple_of(source * pad, pad), pad)
            for x in range(local):
                for half in range(CORES):
                    floats = arrived[CORES * k + half, source, x * pad:(x + 1) * pad, :].astype(F32)
                    squares[x, place, :] += floats * floats
                    normed[x, place, half * shard:(half + 1) * shard] = (
                        floats * gain[CORES * k + half]).astype(BF16)

        loop(0, n_ep, prepare)
        depth = pl.ds(pl.multiple_of(k * deep, deep), deep)
        for x in range(local):
            gate_sum[x] += dot(normed[x], gate[x, depth, :])
            up_sum[x] += dot(normed[x], up[x, depth, :])

    def visit(i, action):
        k = z - (i + 1) // 2 * (i % 2) + i // 2 * (1 - i % 2)

        @pl.when((k >= 0) & (k < nz))
        def _():
            action(k)

    def arrival(i):
        @pl.when(i < 2 * nz - 1)
        def _():
            visit(i, pass_on)

        @pl.when(i >= 2)
        def _():
            visit(i - 2, absorb)

    with jax.named_scope("absorb"):
        loop(0, 2 * nz + 1, arrival)

    with jax.named_scope("picks"):
        pick_tables()

    count = n_ep * pad

    def goal(i):
        return jnp.where(2 * z < nz, nz - 1 - i, i)

    def pair_copy(k):
        return send(part.at[1 - c, k], pair.at[k], pr_s.at[k], pr_r.at[k], (e, partner))

    def exchange(k, d):
        target = (e + d) % n_ep
        return send(fin.at[k, target], ex.at[k, e], ex_s.at[k, d - 1], ex_r.at[k, d - 1], (target, t))

    def exchanged(k, d):
        origin = (e + n_ep - d) % n_ep
        return send(fin.at[k, origin], ex.at[k, origin], ex_s.at[k, d - 1], ex_r.at[k, d - 1],
                    (origin, t))

    def slot_copy(way):
        k = z + 1 if way == 0 else z - 1
        target = t + CORES if way == 0 else t - CORES
        return send(fin.at[k], slot_got.at[way], sl_s.at[way], sl_r.at[way], (e, target))

    def slot_recv(way):
        return send(fin.at[z], slot_got.at[way], sl_s.at[way], sl_r.at[way], (e, partner))

    def token_copy(k):
        return send(tok_stage.at[k], tok_got.at[z], tk_s.at[k], tk_r.at[z], (e, CORES * k + c))

    def token_got(k):
        return send(tok_stage.at[k], tok_got.at[k], tk_s.at[k], tk_r.at[k], (e, CORES * k + c))

    def is_far(k):
        return (k > z + 1) | (k < z - 1)

    with jax.named_scope("hidden"):
        for x in range(local):
            mean = jnp.sum(squares[x], axis=1, keepdims=True) / width_total
            factor = lax.rsqrt(mean + NORM_EPS)
            gate_pre = jnp.minimum(gate_sum[x] * factor, CLAMP_LIMIT)
            up_pre = jnp.clip(up_sum[x] * factor, -CLAMP_LIMIT, CLAMP_LIMIT)
            hidden[x] = ((up_pre + 1.0) * gate_pre * jax.nn.sigmoid(GLU_ALPHA * gate_pre)).astype(BF16)

    def project(i):
        k = goal(i)
        place = pl.ds(pl.multiple_of(k * deep, deep), deep)
        for x in range(local):
            product = dot(hidden[x], down[x, :, place]).astype(BF16)
            for half in range(CORES):
                part[half, k, x] = product[:, half * shard:(half + 1) * shard]
        pair_copy(k).start()

    def finish(i):
        k = goal(i)
        pair_copy(k).wait_recv()
        for x in range(local):
            both = (part[c, k, x].astype(F32) + pair[k, x].astype(F32)).astype(BF16)
            for source in range(n_ep):
                fin[k, source, x * pad:(x + 1) * pad, :] = both[source * pad:(source + 1) * pad, :]

        @pl.when(is_far(k))
        def _():
            loop(1, n_ep, lambda d: exchange(k, d).start())

        @pl.when(k == z + 1)
        def _():
            slot_copy(0).start()

        @pl.when(k == z - 1)
        def _():
            slot_copy(1).start()

    with jax.named_scope("project"):
        loop(0, nz, project)
    with jax.named_scope("finish"):
        loop(0, nz, finish)

    def mixture(results):
        mixed = None
        for p in range(picks):
            selected = dot(pick[p], results)
            weight = jnp.concatenate([pick_w[p]] * (shard // 128), axis=1)
            mixed = selected * weight if mixed is None else mixed + selected * weight
        return mixed

    def tokens_out(i):
        k = goal(i)

        @pl.when(is_far(k))
        def _():
            ex[k, e] = fin[k, e]
            loop(1, n_ep, lambda d: exchanged(k, d).wait_recv())
            tok_stage[k] = mixture(ex[k].reshape(slots, shard)).astype(BF16)
            token_copy(k).start()

    third = (n_ep - 1 + 2) // 3
    with jax.named_scope("far0"):
        attend_far(0, third)
    with jax.named_scope("tokens_out"):
        loop(0, nz, tokens_out)
    with jax.named_scope("slots_in"):
        @pl.when(has_dn)
        def _():
            slot_recv(0).wait_recv()

        @pl.when(has_up)
        def _():
            slot_recv(1).wait_recv()

        for x in range(local):
            span = slice(x * pad, (x + 1) * pad)
            for source in range(n_ep):
                total = fin[z, source, span, :].astype(F32)
                low = slot_got[0, source, span, :].astype(F32)
                high = slot_got[1, source, span, :].astype(F32)
                total = total + jnp.where(has_dn, low, 0.0) + jnp.where(has_up, high, 0.0)
                final[source, span, :] = total.astype(BF16)

    def give(d):
        return send(final.at[(e + d) % n_ep], back.at[e], rt_s.at[d - 1], rt_r.at[d - 1],
                    ((e + d) % n_ep, t))

    def given(d):
        origin = (e + n_ep - d) % n_ep
        return send(final.at[origin], back.at[origin], rt_s.at[d - 1], rt_r.at[d - 1], (origin, t))

    loop(1, n_ep, lambda d: give(d).start())
    back[e] = final[e]

    with jax.named_scope("far1"):
        attend_far(third, 2 * third)
    with jax.named_scope("far2"):
        attend_far(2 * third, n_ep)
    with jax.named_scope("attn_fin"):
        for h in range(heads):
            first = weighted[2 * h] / norm_sum[2 * h]
            second = weighted[2 * h + 1] / norm_sum[2 * h + 1]
            blend = first - mix[h] * second
            mean = jnp.mean(blend * blend, axis=1, keepdims=True)
            scaled = (blend * lax.rsqrt(mean + SUB_EPS) * sub_gain[...] * OUT_SCALE).astype(BF16)
            put_i = lax.broadcasted_iota(jnp.int32, (items * heads, items), 0)
            of_i = lax.broadcasted_iota(jnp.int32, (items * heads, items), 1)
            placed = dot((put_i == of_i * heads + h).astype(F32).astype(BF16), scaled)
            woven = placed if h == 0 else woven + placed
        attn_out[...] = woven.astype(BF16)

    with jax.named_scope("send_waits"):
        for r in range(nz - 1):
            shard_send_waits(r)
        loop(0, nz, lambda k: loop(1, n_ep, lambda d: piece(k, d).wait_send()))
        loop(0, nz, lambda k: loop(0, n_ep, lambda d: forward(k, d).wait_send()))
        for d in range(1, n_ep):
            kv_direct(d, lambda copy: copy.wait_send())
        kv_cross(lambda copy: copy.wait_send())
        if relay:
            for origin in range(2):
                kv_pass(origin, lambda copy: copy.wait_send())
        loop(0, nz, lambda k: pair_copy(k).wait_send())

        def far_waits(k):
            @pl.when(is_far(k))
            def _():
                loop(1, n_ep, lambda d: exchange(k, d).wait_send())
                token_copy(k).wait_send()

        loop(0, nz, far_waits)

        @pl.when(has_up)
        def _():
            slot_copy(0).wait_send()

        @pl.when(has_dn)
        def _():
            slot_copy(1).wait_send()

    with jax.named_scope("tokens_in"):
        held_sum[...] = jnp.zeros_like(held_sum)

        def add_far(k):
            @pl.when(is_far(k))
            def _():
                token_got(k).wait_recv()
                held_sum[...] += tok_got[k].astype(F32)

        loop(0, nz, add_far)

    with jax.named_scope("given_wait"):
        loop(1, n_ep, lambda d: given(d).wait_recv())
    with jax.named_scope("combine"):
        moe_out[...] = (mixture(back[...].reshape(slots, shard)) + held_sum[...]).astype(BF16)
        loop(1, n_ep, lambda d: give(d).wait_send())


def make_shards(n_ep, n_tp):
    def shards(
        queries, keys, values, mix_weight, sub_gain, tokens, routes, route_weights,
        expert_gain, gate_weight, up_weight, down_weight,
    ):
        rows, shard = tokens.shape
        picks = routes.shape[1]
        local, depth, units = gate_weight.shape
        cap = 3 * rows * picks // (2 * n_ep * local)
        pad = -(-cap // 16) * 16
        length, heads, width = queries.shape
        value_width = values.shape[2]
        nz = n_tp // CORES
        block = local * pad
        count = n_ep * pad
        vmem = pl.BlockSpec(memory_space=pltpu.VMEM)
        hbm = pl.BlockSpec(memory_space=pltpu.HBM)
        dma = pltpu.SemaphoreType.DMA
        peers = n_ep - 1
        attn, moe = pl.pallas_call(
            functools.partial(layer_kernel, n_ep, n_tp, cap, heads, pad),
            out_shape=(
                pltpu.VMEM((length * heads, value_width), BF16),
                pltpu.VMEM((rows, shard), BF16),
            ),
            in_specs=[hbm] * 11 + [pl.BlockSpec(memory_space=pltpu.SMEM)],
            out_specs=(vmem, vmem),
            scratch_shapes=[
                pltpu.VMEM((rows, shard), BF16),
                pltpu.VMEM((picks, rows), jnp.int32),
                pltpu.VMEM((picks, rows), F32),
                pltpu.VMEM((n_tp, 1, shard), F32),
                pltpu.VMEM((length * heads, width), BF16),
                pltpu.VMEM((length * heads, width), BF16),
                pltpu.VMEM((length * heads, value_width), BF16),
                pltpu.VMEM((1, value_width), F32),
                pltpu.VMEM(gate_weight.shape, BF16),
                pltpu.VMEM(up_weight.shape, BF16),
                pltpu.VMEM(down_weight.shape, BF16),
                pltpu.VMEM((nz, rows, shard), BF16),
                pltpu.VMEM((nz, n_ep, block, shard), BF16),
                pltpu.VMEM((n_tp, n_ep, block, shard), BF16),
                pltpu.VMEM((local, count, CORES * shard), BF16),
                pltpu.VMEM((local, count, shard), F32),
                pltpu.VMEM((local, count, units), F32),
                pltpu.VMEM((local, count, units), F32),
                pltpu.VMEM((local, count, units), BF16),
                pltpu.VMEM((CORES, nz, local, count, shard), BF16),
                pltpu.VMEM((nz, local, count, shard), BF16),
                pltpu.VMEM((nz, n_ep, block, shard), BF16),
                pltpu.VMEM((nz, n_ep, block, shard), BF16),
                pltpu.VMEM((2, n_ep, block, shard), BF16),
                pltpu.VMEM((nz, rows, shard), BF16),
                pltpu.VMEM((nz, rows, shard), BF16),
                pltpu.VMEM((rows, shard), F32),
                pltpu.VMEM((n_ep, block, shard), BF16),
                pltpu.VMEM((n_ep, block, shard), BF16),
                pltpu.VMEM((picks, rows, n_ep * block), BF16),
                pltpu.VMEM((picks, rows, 128), F32),
                pltpu.VMEM((heads, length, width), BF16),
                pltpu.VMEM((2, heads, length, width), BF16),
                pltpu.VMEM((n_ep, 2, heads, length, width), BF16),
                pltpu.VMEM((2 * heads, length, 1), F32),
                pltpu.VMEM((2 * heads, length, 1), F32),
                pltpu.VMEM((2 * heads, length, value_width), F32),
                dma((8,)),
                dma((3,)),
                dma((2, nz - 1)), dma((2, nz - 1)),
                dma((nz, peers)), dma((nz, peers)),
                dma((nz, n_ep)), dma((nz, n_ep)),
                dma((max(peers, 2),)), dma((n_ep,)),
                dma((2, 2)), dma((2, 2)),
                dma((nz,)), dma((nz,)),
                dma((nz, peers)), dma((nz, peers)),
                dma((2,)), dma((2,)),
                dma((nz,)), dma((nz,)),
                dma((peers,)), dma((peers,)),
            ],
            compiler_params=pltpu.CompilerParams(
                collective_id=0, has_side_effects=True, vmem_limit_bytes=54 * 2**20),
            name="layer",
        )(*(pltpu.with_memory_space_constraint(x, pltpu.HBM) for x in (
            tokens, jnp.transpose(routes), jnp.transpose(route_weights),
            expert_gain.reshape(n_tp, 1, shard), gate_weight, up_weight, down_weight,
            queries.reshape(length * heads, width), keys.reshape(length * heads, width),
            values.reshape(length * heads, value_width), sub_gain[None, :],
        )), mix_weight)
        return attn.reshape(length, heads, value_width), moe

    return shards


def solution(mesh):
    return jax.shard_map(
        make_shards(mesh.shape["ep"], mesh.shape["tp"]),
        mesh=mesh,
        in_specs=(
            P("ep", "tp", None),
            P("ep", "tp", None),
            P("ep", "tp", None),
            P("tp"),
            P(),
            P("ep", "tp"),
            P("ep", None),
            P("ep", None),
            P(),
            P("ep", None, "tp"),
            P("ep", None, "tp"),
            P("ep", "tp", None),
        ),
        out_specs=(P("ep", "tp", None), P("ep", "tp")),
        check_vma=False,
    )
```

time: 80.7 us -> 63.3 us (0.78)
  the two profiles are of different devices: /device:TPU:18 before, /device:TPU:14 now
where the time goes in v1:
time: 63.3 us; the launch traced here: 63.2 us
  Pallas kernels  61.2 us (97%)
  local copies, waits for them, and re-layouts  1.36 us (2%)
  between operations  0.64 us (1%)
    pallas_call x1, Pallas kernels, shards(): pl.pallas_call(functools.partial(layer_kernel, n_ep, n_tp, cap, heads, pa...  61.2 us
    unnamed x2, local copies, waits for them, and re-layouts  1.36 us

profile of v1, /device:TPU:14, one launch (start us, length us, event | category | flops | bytes accessed | tf_op | source)
XLA Modules:
  0.0 63.2 jit_solution(10552351823023585518)
XLA Ops:
  0.6 61.2 %layer.1 = (bf16[1024,128]{1,0:T(8,128)(2,1)S(1)}, bf16[256,256]{1,0:T(8,128)(2,1)S(1)}) custom-call(bf16[256,256]{1,0:T(8,128)(2,1)} %tok_hbm.1, s32[2,256]{1,0:T(2,128)} %bitcast.13, f32[2,256]{1,0:T(2,128)} %bitcast.14, f32[8,1,256]{2,1,0:T(1,128)} %bitcast.12, bf16[2,2048,512]{2,1,0:T(8,128)(2,1)} %gate_hbm.1, bf16[2,2048,512]{2,1,0:T(8,128)(2,1)} %up_hbm.1, ...), custom_call_target="tpu_custom_call" | custom-call | tf_op jit(solution)/shard_map/layer/pallas_call | solution.py:588
  61.8 0.7 %copy.16 = bf16[512,2,128]{2,1,0:T(2,128)(2,1)} copy(bf16[512,2,128]{2,1,0:T(2,128)(2,1)S(1)} %bitcast.8) | data formatting | bytes 524288
  62.5 0.7 %copy.17 = bf16[256,256]{1,0:T(8,128)(2,1)} copy(bf16[256,256]{1,0:T(8,128)(2,1)S(1)} %get-tuple-element.7) | data formatting | bytes 262144

commit v2 on v1

--- a/solution.py
+++ b/solution.py
@@ -14,6 +14,7 @@
 GLU_ALPHA = 1.702
 OUT_SCALE = 0.8
 CORES = 2
+LANES = 128
 F32 = jnp.float32
 BF16 = jnp.bfloat16
 MESH = pl.DeviceIdType.MESH
@@ -166,7 +167,7 @@
         loop(1, n_ep, lambda d: piece(k, d).start())
         forward(k, 0).start()
 
-    items = q.shape[1]
+    items, width = q.shape[1:]
 
     def unpack():
         for copy in loads[2:]:
@@ -175,7 +176,11 @@
         from_i = lax.broadcasted_iota(jnp.int32, (items, items * heads), 1)
         for h in range(heads):
             take = (from_i == pick_i * heads + h).astype(F32).astype(BF16)
-            q[h] = dot(take, q_in[...]).astype(BF16)
+            scaled_q = dot(take, q_in[...]) * (width // 2) ** -0.5
+            lane = lax.broadcasted_iota(jnp.int32, (items, width), 1)
+            for m in range(2):
+                mine = (lane < width // 2) if m == 0 else (lane >= width // 2)
+                q[2 * h + m] = jnp.where(mine, scaled_q, 0.0).astype(BF16)
             kv[0, h] = dot(take, k_in[...]).astype(BF16)
             kv[1, h] = dot(take, v_in[...]).astype(BF16)
 
@@ -185,34 +190,37 @@
             pick[p] = (lane_slot == as_column(slot_row[p])).astype(F32).astype(BF16)
             pick_w[p] = jnp.transpose(jnp.broadcast_to(route_w_t[p:p + 1, :], (128, rows)))
 
-    length, width = q.shape[1:]
-    lane = lax.broadcasted_iota(jnp.int32, (length, width), 1)
-    scale = (width // 2) ** -0.5
+    length = items
+    value_width = kv.shape[3]
+    ones = jnp.ones((length, LANES), BF16)
+
+    def across(column, lanes):
+        return jnp.concatenate([column] * (lanes // LANES), axis=1)
 
     def attend(keys_values, diagonal):
         for h in range(heads):
-            key, value = keys_values[0, h], keys_values[1, h]
-            scaled_q = q[h].astype(F32) * scale
+            key = keys_values[0, h]
+            value = jnp.concatenate([keys_values[1, h], ones], axis=1)
             for m in range(2):
                 n = 2 * h + m
-                mine = (lane < width // 2) if m == 0 else (lane >= width // 2)
-                query = jnp.where(mine, scaled_q, 0.0).astype(BF16)
-                scores = dot_t(query, key)
+                scores = dot_t(q[n], key)
                 if diagonal:
                     q_pos = lax.broadcasted_iota(jnp.int32, scores.shape, 0)
                     k_pos = lax.broadcasted_iota(jnp.int32, scores.shape, 1)
                     scores = jnp.where(k_pos <= q_pos, scores, NEG_FILL)
                 high = jnp.max(scores, axis=1, keepdims=True)
-                if not diagonal:
+                if diagonal:
+                    high = jnp.broadcast_to(high, (length, LANES))
+                else:
                     old = top[n]
                     high = jnp.maximum(high, old)
                     shrink = jnp.exp(old - high)
-                w = jnp.exp(scores - high)
-                s = jnp.sum(w, axis=1, keepdims=True)
-                v = dot(w.astype(BF16), value)
+                w = jnp.exp(scores - across(high, length)).astype(BF16)
+                both = dot(w, value)
+                v, s = both[:, :value_width], both[:, value_width:]
                 top[n] = high
                 norm_sum[n] = s if diagonal else norm_sum[n] * shrink + s
-                weighted[n] = v if diagonal else weighted[n] * shrink + v
+                weighted[n] = v if diagonal else weighted[n] * across(shrink, value_width) + v
 
     relay = n_ep == 4
 
@@ -222,40 +230,51 @@
     def kv_got(origin):
         return send(kv, kv_all.at[origin], kv_s.at[0], kv_r.at[origin], (origin, t))
 
-    def kv_direct(d, action):
-        if relay and d == 1:
+    def kv_half(origin, half, device, own=False):
+        place = kv_all.at[origin, half]
+        return send(kv.at[half] if own else place, place, kh_s.at[origin, half],
+                    kh_r.at[origin, half], (device, t))
+
+    def kv_early(action):
+        if relay:
             @pl.when(e % 2 == 0)
             def _():
-                action(kv_copy(d))
-        elif relay and d == 2:
-            @pl.when(e < 2)
-            def _():
-                action(kv_copy(d))
-        elif not relay:
-            @pl.when(e + d < n_ep)
-            def _():
-                action(kv_copy(d))
-
-    def kv_half(origin, half, device):
-        place = kv_all.at[origin, half]
-        return send(place, place, kh_s.at[origin, half], kh_r.at[origin, half], (device, t))
-
-    def kv_cross(action):
+                action(kv_copy(1))
+
+            @pl.when(e == 1)
+            def _():
+                action(kv_copy(2))
+        else:
+            loop(1, n_ep - e, lambda d: action(kv_copy(d)))
+
+    def kv_middle(action):
         if relay:
-            @pl.when(e == 1)
-            def _():
-                action(send(kv.at[0], kv_all.at[1, 0], kh_s.at[1, 0], kh_r.at[1, 0], (2, t)))
+            @pl.when(e == 0)
+            def _():
+                action(kv_half(0, 1, 2, True))
+
+    def kv_late(action):
+        if relay:
+            @pl.when(e == 0)
+            def _():
+                action(kv_half(0, 0, 2, True))
+
+    def kv_second(action):
+        if relay:
+            @pl.when(e == 2)
+            def _():
+                action(kv_half(0, 1, 3))
 
     def kv_pass(origin, action):
         if relay:
-            for half in range(2):
-                @pl.when((e == half + 1) & (origin == 0))
-                def _():
-                    action(kv_half(0, half, 3))
+            @pl.when((e == 1) & (origin == 0))
+            def _():
+                action(kv_half(0, 0, 3))
 
             @pl.when((e == 3) & (origin == 1))
             def _():
-                action(kv_half(1, 1, 2))
+                for half in range(2):
+                    action(kv_half(1, half, 2))
 
     def far_origin(j):
         if relay:
@@ -266,12 +285,15 @@
         def body(j):
             origin = far_origin(j)
             if relay:
-                halves = ((e == 3) & (origin == 0)) | ((e == 2) & (origin == 1))
+                halves = (e == 2) | ((e == 3) & (origin == 0))
 
                 @pl.when(halves)
                 def _():
-                    for half in range(2):
-                        kv_half(origin, half, 3).wait_recv()
+                    kv_half(origin, 0, 3).wait_recv()
+
+                @pl.when(halves & ((e == 3) | (origin == 1)))
+                def _():
+                    kv_half(origin, 1, 3).wait_recv()
 
                 @pl.when(jnp.logical_not(halves))
                 def _():
@@ -315,9 +337,9 @@
         if r == 0:
             with jax.named_scope("diag"):
                 attend(kv, True)
-    for d in range(1, n_ep):
-        kv_direct(d, lambda copy: copy.start())
-    kv_cross(lambda copy: copy.start())
+                pick_tables()
+
+    kv_early(lambda copy: copy.start())
 
     def pass_on(k):
         def body(d):
@@ -364,6 +386,10 @@
         def _():
             visit(i, pass_on)
 
+        @pl.when(i == 2 * nz - 2)
+        def _():
+            kv_middle(lambda copy: copy.start())
+
         @pl.when(i >= 2)
         def _():
             visit(i - 2, absorb)
@@ -371,13 +397,13 @@
     with jax.named_scope("absorb"):
         loop(0, 2 * nz + 1, arrival)
 
-    with jax.named_scope("picks"):
-        pick_tables()
-
     count = n_ep * pad
 
     def goal(i):
-        return jnp.where(2 * z < nz, nz - 1 - i, i)
+        down, up_to = nz - 1 - i, i
+        down = jnp.where(down <= z, down - 1, down)
+        up_to = jnp.where(up_to >= z, up_to + 1, up_to)
+        return jnp.where(i == nz - 1, z, jnp.where(2 * z < nz, down, up_to))
 
     def pair_copy(k):
         return send(part.at[1 - c, k], pair.at[k], pr_s.at[k], pr_r.at[k], (e, partner))
@@ -445,10 +471,18 @@
         def _():
             slot_copy(1).start()
 
-    with jax.named_scope("project"):
-        loop(0, nz, project)
+    def step(i):
+        @pl.when(i < nz)
+        def _():
+            project(i)
+
+        @pl.when(i >= 2)
+        def _():
+            finish(i - 2)
+
     with jax.named_scope("finish"):
-        loop(0, nz, finish)
+        loop(0, nz + 2, step)
+        kv_late(lambda copy: copy.start())
 
     def mixture(results):
         mixed = None
@@ -468,9 +502,16 @@
             tok_stage[k] = mixture(ex[k].reshape(slots, shard)).astype(BF16)
             token_copy(k).start()
 
-    third = (n_ep - 1 + 2) // 3
+    early = jnp.where(e == 2, 0, e) if relay else 0
+    early = jnp.minimum(early, 2)
+    with jax.named_scope("second"):
+        if relay:
+            @pl.when(e == 2)
+            def _():
+                kv_half(0, 1, 3).wait_recv()
+                kv_half(0, 1, 3).start()
     with jax.named_scope("far0"):
-        attend_far(0, third)
+        attend_far(0, early)
     with jax.named_scope("tokens_out"):
         loop(0, nz, tokens_out)
     with jax.named_scope("slots_in"):
@@ -502,14 +543,12 @@
     loop(1, n_ep, lambda d: give(d).start())
     back[e] = final[e]
 
-    with jax.named_scope("far1"):
-        attend_far(third, 2 * third)
     with jax.named_scope("far2"):
-        attend_far(2 * third, n_ep)
+        attend_far(early, n_ep)
     with jax.named_scope("attn_fin"):
         for h in range(heads):
-            first = weighted[2 * h] / norm_sum[2 * h]
-            second = weighted[2 * h + 1] / norm_sum[2 * h + 1]
+            first, second = (
+                weighted[n] / across(norm_sum[n], value_width) for n in (2 * h, 2 * h + 1))
             blend = first - mix[h] * second
             mean = jnp.mean(blend * blend, axis=1, keepdims=True)
             scaled = (blend * lax.rsqrt(mean + SUB_EPS) * sub_gain[...] * OUT_SCALE).astype(BF16)
@@ -524,12 +563,6 @@
             shard_send_waits(r)
         loop(0, nz, lambda k: loop(1, n_ep, lambda d: piece(k, d).wait_send()))
         loop(0, nz, lambda k: loop(0, n_ep, lambda d: forward(k, d).wait_send()))
-        for d in range(1, n_ep):
-            kv_direct(d, lambda copy: copy.wait_send())
-        kv_cross(lambda copy: copy.wait_send())
-        if relay:
-            for origin in range(2):
-                kv_pass(origin, lambda copy: copy.wait_send())
         loop(0, nz, lambda k: pair_copy(k).wait_send())
 
         def far_waits(k):
@@ -564,6 +597,11 @@
     with jax.named_scope("combine"):
         moe_out[...] = (mixture(back[...].reshape(slots, shard)) + held_sum[...]).astype(BF16)
         loop(1, n_ep, lambda d: give(d).wait_send())
+        for part_of in (kv_early, kv_middle, kv_late, kv_second):
+            part_of(lambda copy: copy.wait_send())
+        if relay:
+            for origin in range(2):
+                kv_pass(origin, lambda copy: copy.wait_send())
 
 
 def make_shards(n_ep, n_tp):
@@ -625,11 +663,11 @@
                 pltpu.VMEM((n_ep, block, shard), BF16),
                 pltpu.VMEM((picks, rows, n_ep * block), BF16),
                 pltpu.VMEM((picks, rows, 128), F32),
-                pltpu.VMEM((heads, length, width), BF16),
+                pltpu.VMEM((2 * heads, length, width), BF16),
                 pltpu.VMEM((2, heads, length, width), BF16),
                 pltpu.VMEM((n_ep, 2, heads, length, width), BF16),
-                pltpu.VMEM((2 * heads, length, 1), F32),
-                pltpu.VMEM((2 * heads, length, 1), F32),
+                pltpu.VMEM((2 * heads, length, LANES), F32),
+                pltpu.VMEM((2 * heads, length, LANES), F32),
                 pltpu.VMEM((2 * heads, length, value_width), F32),
                 dma((8,)),
                 dma((3,)),

time: 63.3 us -> 60.1 us (0.949)
  the two profiles are of different devices: /device:TPU:14 before, /device:TPU:0 now
where the time goes in v2:
time: 60.1 us; the launch traced here: 59.9 us
  Pallas kernels  57.9 us (96%)
  local copies, waits for them, and re-layouts  1.36 us (2%)
  between operations  0.64 us (1%)
    pallas_call x1, Pallas kernels, shards(): pl.pallas_call(functools.partial(layer_kernel, n_ep, n_tp, cap, heads, pa...  57.9 us
    unnamed x2, local copies, waits for them, and re-layouts  1.36 us

profile of v2, /device:TPU:0, one launch (start us, length us, event | category | flops | bytes accessed | tf_op | source)
XLA Modules:
  0.0 59.9 jit_solution(6796803838414873902)
XLA Ops:
  0.6 57.9 %layer.1 = (bf16[1024,128]{1,0:T(8,128)(2,1)S(1)}, bf16[256,256]{1,0:T(8,128)(2,1)S(1)}) custom-call(bf16[256,256]{1,0:T(8,128)(2,1)} %tok_hbm.1, s32[2,256]{1,0:T(2,128)} %bitcast.13, f32[2,256]{1,0:T(2,128)} %bitcast.14, f32[8,1,256]{2,1,0:T(1,128)} %bitcast.12, bf16[2,2048,512]{2,1,0:T(8,128)(2,1)} %gate_hbm.1, bf16[2,2048,512]{2,1,0:T(8,128)(2,1)} %up_hbm.1, ...), custom_call_target="tpu_custom_call" | custom-call | tf_op jit(solution)/shard_map/layer/pallas_call | solution.py:626
  58.6 0.7 %copy.16 = bf16[512,2,128]{2,1,0:T(2,128)(2,1)} copy(bf16[512,2,128]{2,1,0:T(2,128)(2,1)S(1)} %bitcast.8) | data formatting | bytes 524288
  59.3 0.7 %copy.17 = bf16[256,256]{1,0:T(8,128)(2,1)} copy(bf16[256,256]{1,0:T(8,128)(2,1)S(1)} %get-tuple-element.7) | data formatting | bytes 262144

commit v3 on v2

--- a/solution.py
+++ b/solution.py
@@ -45,7 +45,7 @@
     gate, up, down, held, outgoing, arrived, normed, squares, gate_sum, up_sum, hidden, part, pair,
     fin, ex, slot_got, tok_stage, tok_got, held_sum, final, back, pick, pick_w, q, kv, kv_all,
     top, norm_sum, weighted,
-    in_sem, w_sem, ag_s, ag_r, dp_s, dp_r, fw_s, fw_r, kv_s, kv_r, kh_s, kh_r, pr_s, pr_r,
+    in_sem, w_sem, ag_s, ag_r, dp_s, dp_r, fw_s, fw_r, kv_s, kv_r, kh_s, kh_r, kq_s, kq_r, pr_s, pr_r,
     ex_s, ex_r, sl_s, sl_r, tk_s, tk_r, rt_s, rt_r,
 ):
     e, t = lax.axis_index("ep"), lax.axis_index("tp")
@@ -259,12 +259,25 @@
             def _():
                 action(kv_half(0, 0, 2, True))
 
+            if near:
+                @pl.when(e == 1)
+                def _():
+                    action(kv_heads(True))
+
     def kv_second(action):
         if relay:
             @pl.when(e == 2)
             def _():
                 action(kv_half(0, 1, 3))
 
+    near = heads // 2
+
+    def kv_heads(own):
+        span = pl.ds(0, near) if own else pl.ds(near, heads - near)
+        place = kv_all.at[1, 1, span]
+        index = 0 if own else 1
+        return send(kv.at[1, span] if own else place, place, kq_s.at[index], kq_r.at[index], (2, t))
+
     def kv_pass(origin, action):
         if relay:
             @pl.when((e == 1) & (origin == 0))
@@ -273,8 +286,8 @@
 
             @pl.when((e == 3) & (origin == 1))
             def _():
-                for half in range(2):
-                    action(kv_half(1, half, 2))
+                action(kv_half(1, 0, 2))
+                action(kv_heads(False))
 
     def far_origin(j):
         if relay:
@@ -291,9 +304,15 @@
                 def _():
                     kv_half(origin, 0, 3).wait_recv()
 
-                @pl.when(halves & ((e == 3) | (origin == 1)))
+                @pl.when(halves & (e == 3))
                 def _():
                     kv_half(origin, 1, 3).wait_recv()
+
+                @pl.when(halves & (e == 2) & (origin == 1))
+                def _():
+                    kv_heads(False).wait_recv()
+                    if near:
+                        kv_heads(True).wait_recv()
 
                 @pl.when(jnp.logical_not(halves))
                 def _():
@@ -602,6 +621,17 @@
         if relay:
             for origin in range(2):
                 kv_pass(origin, lambda copy: copy.wait_send())
+
+
+def store_kernel(attn, moe, attn_hbm, moe_hbm, sems):
+    copies = [
+        pltpu.make_async_copy(source, target, sems.at[i])
+        for i, (source, target) in enumerate(((attn, attn_hbm), (moe, moe_hbm)))
+    ]
+    for copy in copies:
+        copy.start()
+    for copy in copies:
+        copy.wait()
 
 
 def make_shards(n_ep, n_tp):
@@ -676,6 +706,7 @@
                 dma((nz, n_ep)), dma((nz, n_ep)),
                 dma((max(peers, 2),)), dma((n_ep,)),
                 dma((2, 2)), dma((2, 2)),
+                dma((2,)), dma((2,)),
                 dma((nz,)), dma((nz,)),
                 dma((nz, peers)), dma((nz, peers)),
                 dma((2,)), dma((2,)),
@@ -691,6 +722,18 @@
             queries.reshape(length * heads, width), keys.reshape(length * heads, width),
             values.reshape(length * heads, value_width), sub_gain[None, :],
         )), mix_weight)
+        attn, moe = pl.pallas_call(
+            store_kernel,
+            out_shape=(
+                jax.ShapeDtypeStruct((length * heads, value_width), BF16),
+                jax.ShapeDtypeStruct((rows, shard), BF16),
+            ),
+            in_specs=[vmem, vmem],
+            out_specs=(hbm, hbm),
+            scratch_shapes=[dma((2,))],
+            compiler_params=pltpu.CompilerParams(vmem_limit_bytes=4 * 2**20),
+            name="store",
+        )(attn, moe)
         return attn.reshape(length, heads, value_width), moe
 
     return shards

time: 60.1 us -> 56.8 us (0.945)
  Pallas kernels: 57.9 us -> 55.9 us
  local copies, waits for them, and re-layouts: 1.36 us -> 0 us
    pallas_call x1, Pallas kernels: 57.9 us -> 55.1 us  [shards(): pl.pallas_call(functools.partial(layer_kernel, n_ep, n_tp, cap, heads, pa...]
    unnamed x2 -> x0, local copies, waits for them, and re-layouts: 1.36 us -> none
    pallas_call x0 -> x1, Pallas kernels: none -> 0.76 us  [shards(): pl.pallas_call(store_kernel, out_shape=(jax.ShapeDtypeStruct((length * he...]
where the time goes in v3:
time: 56.8 us; the launch traced here: 56.6 us
  Pallas kernels  55.9 us (98%)
  between operations  0.64 us (1%)
    pallas_call x1, Pallas kernels, shards(): pl.pallas_call(functools.partial(layer_kernel, n_ep, n_tp, cap, heads, pa...  55.1 us

profile of v3, /device:TPU:0, one launch (start us, length us, event | category | flops | bytes accessed | tf_op | source)
XLA Modules:
  0.0 56.6 jit_solution(2218741468203469251)
XLA Ops:
  0.6 55.1 %layer.1 = (bf16[1024,128]{1,0:T(8,128)(2,1)S(1)}, bf16[256,256]{1,0:T(8,128)(2,1)S(1)}) custom-call(bf16[256,256]{1,0:T(8,128)(2,1)} %tok_hbm.1, s32[2,256]{1,0:T(2,128)} %bitcast.12, f32[2,256]{1,0:T(2,128)} %bitcast.13, f32[8,1,256]{2,1,0:T(1,128)} %bitcast.11, bf16[2,2048,512]{2,1,0:T(8,128)(2,1)} %gate_hbm.1, bf16[2,2048,512]{2,1,0:T(8,128)(2,1)} %up_hbm.1, ...), custom_call_target="tpu_custom_call" | custom-call | tf_op jit(solution)/shard_map/layer/pallas_call | solution.py:656
  55.8 0.8 %store.1 = (bf16[1024,128]{1,0:T(8,128)(2,1)}, bf16[256,256]{1,0:T(8,128)(2,1)}) custom-call(bf16[1024,128]{1,0:T(8,128)(2,1)S(1)} %get-tuple-element.6.attn, bf16[256,256]{1,0:T(8,128)(2,1)S(1)} %get-tuple-element.7.moe), custom_call_target="tpu_custom_call" | custom-call | tf_op jit(solution)/shard_map/store/pallas_call | solution.py:725

commit v4 on v3

--- a/solution.py
+++ b/solution.py
@@ -39,9 +39,9 @@
 def layer_kernel(
     n_ep, n_tp, cap, heads, rank_pad,
     tok_hbm, routes_hbm, route_w_hbm, gain_hbm, gate_hbm, up_hbm, down_hbm,
-    q_hbm, k_hbm, v_hbm, sub_gain_hbm, mix,
+    q_hbm, k_hbm, v_hbm, sub_gain_hbm, mix_hbm,
     attn_out, moe_out,
-    tok, routes_t, route_w_t, gain, q_in, k_in, v_in, sub_gain,
+    tok, routes_t, route_w_t, gain, q_in, k_in, v_in, sub_gain, mix,
     gate, up, down, held, outgoing, arrived, normed, squares, gate_sum, up_sum, hidden, part, pair,
     fin, ex, slot_got, tok_stage, tok_got, held_sum, final, back, pick, pick_w, q, kv, kv_all,
     top, norm_sum, weighted,
@@ -64,7 +64,7 @@
         pltpu.make_async_copy(source, target, in_sem.at[i])
         for i, (source, target) in enumerate((
             (tok_hbm, tok), (routes_hbm, routes_t), (route_w_hbm, route_w_t), (gain_hbm, gain),
-            (q_hbm, q_in), (k_hbm, k_in), (v_hbm, v_in), (sub_gain_hbm, sub_gain)))
+            (q_hbm, q_in), (k_hbm, k_in), (v_hbm, v_in), (sub_gain_hbm, sub_gain), (mix_hbm, mix)))
     ]
     for copy in loads:
         copy.start()
@@ -562,43 +562,33 @@
     loop(1, n_ep, lambda d: give(d).start())
     back[e] = final[e]
 
+    with jax.named_scope("early_waits"):
+        for r in range(nz - 1):
+            shard_send_waits(r)
+        loop(0, nz, lambda k: loop(1, n_ep, lambda d: piece(k, d).wait_send()))
+        loop(0, nz, lambda k: loop(0, n_ep, lambda d: forward(k, d).wait_send()))
+        loop(0, nz, lambda k: pair_copy(k).wait_send())
+
     with jax.named_scope("far2"):
         attend_far(early, n_ep)
     with jax.named_scope("attn_fin"):
+        finished = []
         for h in range(heads):
             first, second = (
                 weighted[n] / across(norm_sum[n], value_width) for n in (2 * h, 2 * h + 1))
             blend = first - mix[h] * second
             mean = jnp.mean(blend * blend, axis=1, keepdims=True)
             scaled = (blend * lax.rsqrt(mean + SUB_EPS) * sub_gain[...] * OUT_SCALE).astype(BF16)
-            put_i = lax.broadcasted_iota(jnp.int32, (items * heads, items), 0)
-            of_i = lax.broadcasted_iota(jnp.int32, (items * heads, items), 1)
-            placed = dot((put_i == of_i * heads + h).astype(F32).astype(BF16), scaled)
-            woven = placed if h == 0 else woven + placed
+            finished.append(scaled)
+        put_i = lax.broadcasted_iota(jnp.int32, (items * heads, items), 0)
+        of_i = lax.broadcasted_iota(jnp.int32, (items * heads, items), 1)
+        spread = (put_i // heads == of_i).astype(F32).astype(BF16)
+        wide = dot(spread, jnp.concatenate(finished, axis=1))
+        head_i = lax.broadcasted_iota(jnp.int32, (items * heads, value_width), 0) % heads
+        woven = wide[:, :value_width]
+        for h in range(1, heads):
+            woven = jnp.where(head_i == h, wide[:, h * value_width:(h + 1) * value_width], woven)
         attn_out[...] = woven.astype(BF16)
-
-    with jax.named_scope("send_waits"):
-        for r in range(nz - 1):
-            shard_send_waits(r)
-        loop(0, nz, lambda k: loop(1, n_ep, lambda d: piece(k, d).wait_send()))
-        loop(0, nz, lambda k: loop(0, n_ep, lambda d: forward(k, d).wait_send()))
-        loop(0, nz, lambda k: pair_copy(k).wait_send())
-
-        def far_waits(k):
-            @pl.when(is_far(k))
-            def _():
-                loop(1, n_ep, lambda d: exchange(k, d).wait_send())
-                token_copy(k).wait_send()
-
-        loop(0, nz, far_waits)
-
-        @pl.when(has_up)
-        def _():
-            slot_copy(0).wait_send()
-
-        @pl.when(has_dn)
-        def _():
-            slot_copy(1).wait_send()
 
     with jax.named_scope("tokens_in"):
         held_sum[...] = jnp.zeros_like(held_sum)
@@ -615,6 +605,22 @@
         loop(1, n_ep, lambda d: given(d).wait_recv())
     with jax.named_scope("combine"):
         moe_out[...] = (mixture(back[...].reshape(slots, shard)) + held_sum[...]).astype(BF16)
+        def far_waits(k):
+            @pl.when(is_far(k))
+            def _():
+                loop(1, n_ep, lambda d: exchange(k, d).wait_send())
+                token_copy(k).wait_send()
+
+        loop(0, nz, far_waits)
+
+        @pl.when(has_up)
+        def _():
+            slot_copy(0).wait_send()
+
+        @pl.when(has_dn)
+        def _():
+            slot_copy(1).wait_send()
+
         loop(1, n_ep, lambda d: give(d).wait_send())
         for part_of in (kv_early, kv_middle, kv_late, kv_second):
             part_of(lambda copy: copy.wait_send())
@@ -659,7 +665,7 @@
                 pltpu.VMEM((length * heads, value_width), BF16),
                 pltpu.VMEM((rows, shard), BF16),
             ),
-            in_specs=[hbm] * 11 + [pl.BlockSpec(memory_space=pltpu.SMEM)],
+            in_specs=[hbm] * 12,
             out_specs=(vmem, vmem),
             scratch_shapes=[
                 pltpu.VMEM((rows, shard), BF16),
@@ -670,6 +676,7 @@
                 pltpu.VMEM((length * heads, width), BF16),
                 pltpu.VMEM((length * heads, value_width), BF16),
                 pltpu.VMEM((1, value_width), F32),
+                pltpu.SMEM((heads,), F32),
                 pltpu.VMEM(gate_weight.shape, BF16),
                 pltpu.VMEM(up_weight.shape, BF16),
                 pltpu.VMEM(down_weight.shape, BF16),
@@ -699,7 +706,7 @@
                 pltpu.VMEM((2 * heads, length, LANES), F32),
                 pltpu.VMEM((2 * heads, length, LANES), F32),
                 pltpu.VMEM((2 * heads, length, value_width), F32),
-                dma((8,)),
+                dma((9,)),
                 dma((3,)),
                 dma((2, nz - 1)), dma((2, nz - 1)),
                 dma((nz, peers)), dma((nz, peers)),
@@ -721,7 +728,7 @@
             expert_gain.reshape(n_tp, 1, shard), gate_weight, up_weight, down_weight,
             queries.reshape(length * heads, width), keys.reshape(length * heads, width),
             values.reshape(length * heads, value_width), sub_gain[None, :],
-        )), mix_weight)
+        )), pltpu.with_memory_space_constraint(mix_weight, pltpu.HBM) if heads > 1 else mix_weight)
         attn, moe = pl.pallas_call(
             store_kernel,
             out_shape=(

time: 56.8 us -> 56.1 us (0.988)
  no operation moved by 1% of the time
where the time goes in v4:
time: 56.1 us; the launch traced here: 56 us
  Pallas kernels  55.4 us (99%)
  between operations  0.64 us (1%)
    pallas_call x1, Pallas kernels, shards(): pl.pallas_call(functools.partial(layer_kernel, n_ep, n_tp, cap, heads, pa...  54.6 us

profile of v4, /device:TPU:0, one launch (start us, length us, event | category | flops | bytes accessed | tf_op | source)
XLA Modules:
  0.0 56.0 jit_solution(8309155800083155949)
XLA Ops:
  0.6 54.6 %layer.1 = (bf16[1024,128]{1,0:T(8,128)(2,1)S(1)}, bf16[256,256]{1,0:T(8,128)(2,1)S(1)}) custom-call(bf16[256,256]{1,0:T(8,128)(2,1)} %tok_hbm.1, s32[2,256]{1,0:T(2,128)} %bitcast.12, f32[2,256]{1,0:T(2,128)} %bitcast.13, f32[8,1,256]{2,1,0:T(1,128)} %bitcast.11, bf16[2,2048,512]{2,1,0:T(8,128)(2,1)} %gate_hbm.1, bf16[2,2048,512]{2,1,0:T(8,128)(2,1)} %up_hbm.1, ...), custom_call_target="tpu_custom_call" | custom-call | tf_op jit(solution)/shard_map/layer/pallas_call | solution.py:662
  55.2 0.8 %store.1 = (bf16[1024,128]{1,0:T(8,128)(2,1)}, bf16[256,256]{1,0:T(8,128)(2,1)}) custom-call(bf16[1024,128]{1,0:T(8,128)(2,1)S(1)} %get-tuple-element.6.attn, bf16[256,256]{1,0:T(8,128)(2,1)S(1)} %get-tuple-element.7.moe), custom_call_target="tpu_custom_call" | custom-call | tf_op jit(solution)/shard_map/store/pallas_call | solution.py:732
